TPU v7x, 32 devices: a whole 2x2x4 slice. The times are simulated.
32 devices in a mesh: sp: 4 (over y, x), tp: 8 (over z, core).
Axes of the slice: x: 2, y: 2, z: 4, core: 2. Of those that a mesh axis runs over, the one named last changes fastest.
Arguments:
- latent: bfloat16 [2048, 4096], P(('sp', 'tp')), may hold values from -6 to 6
- context: bfloat16 [512, 4096], P('sp'), may hold values from -6 to 6
- condition: float32 [4096], replicated, may hold values from -6 to 6
- context_condition: float32 [4096], replicated, may hold values from -6 to 6
- modulation: bfloat16 [3, 4096, 4096], P(None, 'sp', 'tp'), may hold values from -0.09375 to 0.09375
- query_weight: bfloat16 [4096, 4096], P(None, 'tp'), as said below
- key_weight: bfloat16 [4096, 4096], P(None, 'tp'), as said below
- value_weight: bfloat16 [4096, 4096], P(None, 'tp'), may hold values from -0.09375 to 0.09375
- lambdas: float32 [16], P('tp'), may hold values from 0.3 to 0.8
- context_lift: float32 [16], P('tp'), may hold values from 1.5 to 3
- head_gain: float32 [256], replicated, may hold values from 0.1 to 1.9
- output_weight: bfloat16 [4096, 4096], P('tp'), may hold values from -0.09375 to 0.09375
Outputs:
- result: bfloat16 [2048, 4096], P(('sp', 'tp'))
Inputs may be any that keep to these rules, and one draw needn't show every extreme that they name: `query_weight`: entries lie within 200 / sqrt(4096) in magnitude. `key_weight`: entries lie within 6 / sqrt(4096) in magnitude.
All inputs are finite; a program needn't handle non-finite values.
Results may differ from a plain program's by a relative error of at most 0.025.
Values may be sent and summed in bfloat16 or wider, within the bound.
A program may use at most 64 MiB of HBM per device.

v0:
```python
import math

import jax
import jax.numpy as jnp
from jax import lax
from jax.sharding import PartitionSpec as P

GRID_W = 64


ROPE_BASE = 10000.0
EPSILON = 1e-05


def modulate(tokens_in, offset, scaling):
    values = tokens_in.astype(jnp.float32)
    center = jnp.mean(values, axis=-1, keepdims=True)
    spread = jnp.mean(jnp.square(values - center), axis=-1, keepdims=True)
    normed = (values - center) * lax.rsqrt(spread + EPSILON)
    return (normed * (1.0 + scaling) + offset).astype(jnp.bfloat16)


def rotate(tensor, places):
    number, head_count, head_width = tensor.shape
    quarter = head_width // 4
    eighth = head_width // 8
    inverse = ROPE_BASE ** (-jnp.arange(eighth, dtype=jnp.float32) / eighth)
    grid_row = (places // GRID_W).astype(jnp.float32)
    grid_col = (places % GRID_W).astype(jnp.float32)
    angles = jnp.stack([grid_row[:, None] * inverse, grid_col[:, None] * inverse], axis=1)
    cosine = jnp.cos(angles)[:, None, None, :, :]
    sine_table = jnp.sin(angles)[:, None, None, :, :]
    pieces = tensor.reshape(number, head_count, 2, 2, quarter)
    first_half = pieces[..., :eighth]
    second = pieces[..., eighth:]
    turned = jnp.concatenate(
        [first_half * cosine - second * sine_table, second * cosine + first_half * sine_table],
        axis=-1,
    )
    return turned.reshape(number, head_count, head_width)


def absorb(state_in, key_block, queries, lift_term, scale_factor):
    running_max, running_sum, running_out = state_in
    key_count = key_block.shape[0]
    head_count = queries.shape[1]
    head_width = 2 * queries.shape[3]
    local_width = head_count * head_width
    key_part = key_block[:, :local_width].reshape(key_count, head_count, 2, head_width // 2)
    value_part = key_block[:, local_width:].reshape(key_count, head_count, head_width)
    scores = (
        jnp.einsum("qhmd,khmd->mqhk", queries, key_part, preferred_element_type=jnp.float32)
        * scale_factor
        + lift_term
    )
    new_max = jnp.maximum(running_max, jnp.max(scores, axis=-1))
    fading = jnp.exp(running_max - new_max)
    weights = jnp.exp(scores - new_max[..., None])
    new_sum = running_sum * fading + jnp.sum(weights, axis=-1)
    new_out = running_out * fading[..., None] + jnp.einsum(
        "mqhk,khd->mqhd",
        weights.astype(jnp.bfloat16),
        value_part,
        preferred_element_type=jnp.float32,
    )
    return (new_max, new_sum, new_out)


def shards(
    latent,
    context,
    condition,
    context_condition,
    modulation,
    query_weight,
    key_weight,
    value_weight,
    lambdas,
    context_lift,
    head_gain,
    output_weight,
):
    sp_index = lax.axis_index("sp")
    rows_block = modulation.shape[1]
    silu_pair = jax.nn.silu(jnp.stack([condition, context_condition])).astype(jnp.bfloat16)
    own_rows = lax.dynamic_slice_in_dim(silu_pair, sp_index * rows_block, rows_block, 1)
    partial_mod = jnp.einsum(
        "cd,rde->cre", own_rows, modulation, preferred_element_type=jnp.float32
    )
    summed = lax.psum(partial_mod, "sp")
    mod_vectors = lax.all_gather(summed, "tp", axis=2, tiled=True)
    head_count = lambdas.shape[0]
    head_width = query_weight.shape[1] // head_count
    half_width = head_width // 2
    local_width = head_count * head_width
    scale_factor = half_width ** (-0.5)
    normed = modulate(latent, mod_vectors[0, 0], mod_vectors[0, 1])
    projection = jnp.concatenate([query_weight, key_weight, value_weight], axis=1)
    projected = jnp.dot(
        lax.all_gather(normed, "tp", axis=0, tiled=True),
        projection,
        preferred_element_type=jnp.float32,
    ).astype(jnp.bfloat16)
    block_tokens = projected.shape[0]
    places = sp_index * block_tokens + jnp.arange(block_tokens, dtype=jnp.int32)
    queries = rotate(
        projected[:, :local_width]
        .astype(jnp.float32)
        .reshape(block_tokens, head_count, head_width),
        places,
    )
    queries = queries.astype(jnp.bfloat16).reshape(block_tokens, head_count, 2, half_width)
    latent_keys = rotate(
        projected[:, local_width : 2 * local_width]
        .astype(jnp.float32)
        .reshape(block_tokens, head_count, head_width),
        places,
    )
    latent_keys = latent_keys.astype(jnp.bfloat16).reshape(block_tokens, local_width)
    packed = jnp.concatenate([latent_keys, projected[:, 2 * local_width :]], axis=1)
    normed_context = modulate(context, mod_vectors[1, 0], mod_vectors[1, 1])
    own_context = jnp.dot(
        normed_context, projection[:, local_width:], preferred_element_type=jnp.float32
    ).astype(jnp.bfloat16)
    context_packed = lax.all_gather(own_context, "sp", axis=0, tiled=True)
    initial = (
        jnp.full((2, block_tokens, head_count), -jnp.inf, jnp.float32),
        jnp.zeros((2, block_tokens, head_count), jnp.float32),
        jnp.zeros((2, block_tokens, head_count, head_width), jnp.float32),
    )
    state_now = absorb(initial, context_packed, queries, context_lift[:, None], scale_factor)
    segment = lax.all_gather(packed, "sp", axis=0, tiled=True)
    length = segment.shape[0]
    block_len = math.gcd(length, 1024)
    stacked = segment.reshape(length // block_len, block_len, segment.shape[1])

    def one_block(state_step, block_rows):
        return (absorb(state_step, block_rows, queries, 0.0, scale_factor), None)

    running_max, running_sum, running_out = lax.scan(one_block, state_now, stacked)[0]
    means = running_out / running_sum[..., None]
    difference = means[0] - lambdas[None, :, None] * means[1]
    scaled = (
        difference
        * lax.rsqrt(jnp.mean(jnp.square(difference), axis=-1, keepdims=True) + EPSILON)
        * head_gain
    )
    attended = scaled.astype(jnp.bfloat16).reshape(block_tokens, local_width)
    mixture = lax.psum_scatter(
        jnp.dot(attended, output_weight, preferred_element_type=jnp.float32).astype(jnp.bfloat16),
        "tp",
        scatter_dimension=0,
        tiled=True,
    ).astype(jnp.float32)
    return (latent.astype(jnp.float32) + mod_vectors[0, 2] * mixture).astype(jnp.bfloat16)


def solution(mesh):
    in_specs = (
        P(("sp", "tp"), None),
        P("sp", None),
        P(),
        P(),
        P(None, "sp", "tp"),
        P(None, "tp"),
        P(None, "tp"),
        P(None, "tp"),
        P("tp"),
        P("tp"),
        P(),
        P("tp", None),
    )
    out_specs = P(("sp", "tp"), None)
    return jax.shard_map(shards, mesh=mesh, in_specs=in_specs, out_specs=out_specs, check_vma=False)
```

profile of v0, /device:TPU:0, one launch (start us, length us, event | category | flops | bytes accessed | tf_op | source)
XLA Modules:
  0.0 269.9 jit_solution(10086001366930255042)
XLA Ops:
  6.5 1.9 copy-done
  8.4 1.3 fusion.61
  9.7 17.6 %psum.7 = f32[2,3,512]{2,0,1:T(2,128)S(1)} all-reduce(f32[2,3,512]{2,0,1:T(2,128)S(1)} %fusion.61), channel_id=1, replica_groups=mesh['sp'=4,'tp'=8] {'sp'}, use_global_device_ids=true, to_apply=%region_0.1 | all-reduce | flops 3072 | bytes 24576 | tf_op jit(solution)/shard_map/psum | solution.py:90
  27.3 14.1 %all_gather.12 = f32[2,3,4096]{2,0,1:T(2,128)S(1)} all-gather(f32[2,3,512]{2,0,1:T(2,128)S(1)} %psum.7), channel_id=1, replica_groups=mesh['sp'=4,'tp'=8] {'tp'}, dimensions={2}, use_global_device_ids=true | all-gather | bytes 110592 | tf_op jit(solution)/shard_map/all_gather | solution.py:91
  41.5 1.2 convert_reduce_fusion.1
  42.7 1.3 fusion.40
  44.1 2.1 fusion.43
  46.3 1.5 convert_reduce_fusion
  47.7 0.4 fusion.27
  48.2 5.0 %fusion.37 = bf16[128,1024]{1,0:T(8,128)(2,1)} fusion(bf16[4096,512]{1,0:T(8,128)(2,1)} %param.21, bf16[4096,512]{1,0:T(8,128)(2,1)} %param.20, bf16[128,4096]{1,0:T(8,128)(2,1)S(1)} %copy-done.3, f32[4096]{0:T(1024)S(1)} %bitcast.120, f32[4096]{0:T(1024)S(1)} %bitcast.121, f32[128]{0:T(128)S(1)} %add_rsqrt_fusion.2, f32[128]{0:T(128)S(1)} %broadcast_multiply_fusion.3), kind=kOutput, calls=%fused_computation.47 | convolution fusion | flops 1093795840 | bytes 9733120 | tf_op jit(solution)/shard_map/dot_general | solution.py:122
  53.3 1.1 fusion.58
  54.5 37.9 %all-gather.6.cloned.1.call-done = bf16[512,4096]{1,0:T(8,128)(2,1)} async-done(((bf16[64,4096]{1,0:T(8,128)(2,1)}), bf16[512,4096]{1,0:T(8,128)(2,1)}) %all-gather.6.cloned.1.call-update) | async-done | bytes 4194320 | tf_op jit(solution)/shard_map/all_gather | solution.py:100
  92.4 12.5 %fusion.22 = bf16[512,1536]{1,0:T(8,128)(2,1)S(1)} fusion(bf16[512,4096]{1,0:T(8,128)(2,1)} %all-gather.6.cloned.1.call-done, bf16[4096,512]{1,0:T(8,128)(2,1)} %param.21, bf16[4096,512]{1,0:T(8,128)(2,1)} %param.20, bf16[4096,512]{1,0:T(8,128)(2,1)} %param.19), kind=kOutput, calls=%fused_computation.30 | convolution fusion | flops 6480986112 | bytes 18350080 | tf_op jit(solution)/shard_map/dot_general | solution.py:99
  104.9 1.1 slice_convert_fusion
  106.0 0.3 copy.26
  106.3 0.3 copy.32
  106.7 2.0 subtract_convert_fusion
  108.8 0.2 copy.33
  109.0 1.2 pad_maximum_fusion
  110.2 0.2 reduce-scatter.2.cloned.1.call-start
  110.5 9.1 %all-gather.4.cloned.1.call-done = bf16[512,1024]{1,0:T(8,128)(2,1)} async-done(((bf16[128,1024]{1,0:T(8,128)(2,1)}), bf16[512,1024]{1,0:T(8,128)(2,1)}) %all-gather.4.cloned.1.call-update) | async-done | bytes 1048592 | tf_op jit(solution)/shard_map/all_gather | solution.py:125
  119.6 1.3 fusion.77
  121.0 0.2 copy.47
  121.2 1.0 copy.35
  122.3 1.8 bitcast_reduce_fusion.1
  124.0 1.0 fusion.20
  125.1 2.0 bitcast_add_fusion.1
  127.1 46.9 %all-gather.8.cloned.1.call-done = bf16[2048,1024]{1,0:T(8,128)(2,1)} async-done(((bf16[512,1024]{1,0:T(8,128)(2,1)}), bf16[2048,1024]{1,0:T(8,128)(2,1)}) %all-gather.8.cloned.1.call-update) | async-done | bytes 4194320 | tf_op jit(solution)/shard_map/all_gather | solution.py:132
  174.0 28.7 %while.14 = (s32[]{:T(128)}, f32[2,512,2]{1,2,0:T(2,128)S(1)}, f32[2,512,2]{1,2,0:T(2,128)S(1)}, f32[2,512,2,256]{1,3,0,2:T(8,128)}, bf16[2,1024,1024]{2,1,0:T(8...) while((s32[]{:T(128)}, f32[2,512,2]{1,2,0:T(2,128)S(1)}, f32[2,512,2]{1,2,0:T(2,128)S(1)}, ...), condition=%wide.region_10.11_spmd, body=%wide.region_7.10_spmd.sunk | while | flops 1624248320 | bytes 44703824 | solution.py:140
  174.0 3.1 %constant_dynamic-slice_fusion.2 = bf16[1,1024,1024]{2,1,0:T(8,128)(2,1)} fusion(bf16[2,1024,1024]{2,1,0:T(8,128)(2,1)} %get-tuple-element.173, s32[]{:T(128)} %get-tuple-element.162), kind=kLoop, calls=%fused_computation.12.clone.1 | loop fusion | bytes 4194308 | tf_op jit(solution)/shard_map/while/body/jit(dynamic_index_in_dim)/dynamic_slice | solution.py:140
  177.1 2.9 %copy.75 = bf16[1,1024,1024]{1,2,0:T(8,128)(2,1)S(1)} copy(bf16[1,1024,1024]{2,1,0:T(8,128)(2,1)} %constant_dynamic-slice_fusion.2) | data formatting | bytes 4194304 | tf_op jit(solution)/shard_map/while/body/jit(dynamic_index_in_dim)/dynamic_slice | solution.py:140
  180.2 2.4 bitcast_reduce_fusion.3
  182.6 1.6 fusion.96
  184.2 4.2 %bitcast_add_fusion.3 = f32[2,512,2,256]{1,3,0,2:T(8,128)} fusion(f32[2,512,2,256]{1,3,0,2:T(8,128)} %get-tuple-element.165, bf16[1024,2,256,1]{0,2,3,1:T(8,128)(2,1)S(1)} %bitcast.107, bf16[2,512,2,1024]{1,3,2,0:T(8,128)(2,1)S(1)} %get-tuple-element.153, f32[2,512,2]{1,0,2:T(2,128)S(1)} %copy.76), kind=kOutput, calls=%fused_computation.7.clone.1 | convolution fusion | flops 1074790400 | bytes 9445376 | tf_op jit(solution)/shard_map/while/body/eval_jaxpr/mqhk,khd->mqhd/dot_general | solution.py:60
  188.4 3.1 %constant_dynamic-slice_fusion.2 = bf16[1,1024,1024]{2,1,0:T(8,128)(2,1)} fusion(bf16[2,1024,1024]{2,1,0:T(8,128)(2,1)} %get-tuple-element.173, s32[]{:T(128)} %get-tuple-element.162), kind=kLoop, calls=%fused_computation.12.clone.1 | loop fusion | bytes 4194308 | tf_op jit(solution)/shard_map/while/body/jit(dynamic_index_in_dim)/dynamic_slice | solution.py:140
  191.5 2.9 %copy.75 = bf16[1,1024,1024]{1,2,0:T(8,128)(2,1)S(1)} copy(bf16[1,1024,1024]{2,1,0:T(8,128)(2,1)} %constant_dynamic-slice_fusion.2) | data formatting | bytes 4194304 | tf_op jit(solution)/shard_map/while/body/jit(dynamic_index_in_dim)/dynamic_slice | solution.py:140
  194.3 0.2 fusion.95
  194.5 2.4 bitcast_reduce_fusion.3
  196.9 1.6 fusion.96
  198.6 4.2 %bitcast_add_fusion.3 = f32[2,512,2,256]{1,3,0,2:T(8,128)} fusion(f32[2,512,2,256]{1,3,0,2:T(8,128)} %get-tuple-element.165, bf16[1024,2,256,1]{0,2,3,1:T(8,128)(2,1)S(1)} %bitcast.107, bf16[2,512,2,1024]{1,3,2,0:T(8,128)(2,1)S(1)} %get-tuple-element.153, f32[2,512,2]{1,0,2:T(2,128)S(1)} %copy.76), kind=kOutput, calls=%fused_computation.7.clone.1 | convolution fusion | flops 1074790400 | bytes 9445376 | tf_op jit(solution)/shard_map/while/body/eval_jaxpr/mqhk,khd->mqhd/dot_general | solution.py:60
  202.8 1.9 broadcast_divide_fusion
  204.7 0.2 fusion.76
  204.9 0.3 fusion.47
  205.2 0.3 fusion.50
  205.5 1.3 copy-done.2
  206.8 4.3 %convolution_convert_fusion = bf16[512,4096]{1,0:T(8,128)(2,1)} fusion(bf16[512,512]{0,1:T(8,128)(2,1)S(1)} %fusion.50, bf16[512,4096]{1,0:T(8,128)(2,1)S(1)} %copy-done.2), kind=kOutput, calls=%fused_computation.23 | convolution fusion | flops 2149580800 | bytes 8912896 | tf_op jit(solution)/shard_map/dot_general | solution.py:150
  211.2 50.1 %reduce-scatter.2.cloned.1.call-done = bf16[64,4096]{1,0:T(8,128)(2,1)} async-done(((bf16[512,4096]{1,0:T(8,128)(2,1)}), bf16[64,4096]{1,0:T(8,128)(2,1)}) %reduce-scatter.2.cloned.1.call-update) | async-done | bytes 524304 | tf_op jit(solution)/shard_map/reduce_scatter | solution.py:149
  261.3 2.1 fusion.44
  (51 shorter events, 0.9 us)
Async XLA Ops:
  6.5 1.9 copy-start
  6.5 85.9 %all-gather.6.cloned.1.call-start = ((), (), s32[]{:S(2)}) async-start(), calls=%async_computation.2 | async-start | bytes 4718592 | tf_op jit(solution)/shard_map/all_gather | solution.py:100
  9.7 38.0 %copy-start.3 = (bf16[128,4096]{1,0:T(8,128)(2,1)S(1)}, bf16[128,4096]{1,0:T(8,128)(2,1)}, u32[]{:S(2)}) copy-start(bf16[128,4096]{1,0:T(8,128)(2,1)} %param.15) | copy-start | bytes 3145732
  46.2 73.4 %all-gather.4.cloned.1.call-start = ((), (), s32[]{:S(2)}) async-start(), calls=%async_computation.1 | async-start | bytes 1310720 | tf_op jit(solution)/shard_map/all_gather | solution.py:125
  53.2 120.9 %all-gather.8.cloned.1.call-start = ((), (), s32[]{:S(2)}) async-start(), calls=%async_computation.3 | async-start | bytes 5242880 | tf_op jit(solution)/shard_map/all_gather | solution.py:132
  106.7 2.3 copy-start.4
  108.7 1.7 copy-start.7
  108.7 1.8 copy-start.8
  108.8 12.4 %copy-start.5 = (bf16[512,2,2,2,32]{0,4,3,2,1:T(8,128)(2,1)S(1)}, bf16[512,2,2,2,32]{0,4,3,2,1:T(8,128)(2,1)}, u32[]{:S(2)}) copy-start(bf16[512,2,2,2,32]{0,4,3,2,1:T(8,128)(2,1)} %get-tuple-element.86) | copy-start | bytes 786436
  110.2 12.1 %copy-start.6 = (f32[2]{0:T(128)S(1)}, f32[2]{0:T(128)}, u32[]{:S(2)}) copy-start(f32[2]{0:T(128)} %param.23) | copy-start | bytes 28
  110.2 151.1 %reduce-scatter.2.cloned.1.call-start = ((), (), s32[]{:S(2)}) async-start(), calls=%async_computation.4 | async-start | bytes 4718592 | tf_op jit(solution)/shard_map/reduce_scatter | solution.py:149
  204.7 2.2 copy-start.2
  206.8 56.6 %copy-start.1 = (bf16[3,1024,512]{2,1,0:T(8,128)(2,1)S(1)}, bf16[3,1024,512]{2,1,0:T(8,128)(2,1)}, u32[]{:S(2)}) copy-start(bf16[3,1024,512]{2,1,0:T(8,128)(2,1)} %param.18) | copy-start | bytes 9437188
Sparse Core Ops, SparseCore 0:
  46.3 46.0 all-gather.5
  94.2 25.2 all-gather.3
  121.4 52.5 all-gather.7
  211.3 49.9 reduce-scatter.1
where the time goes:
time: 271 us; the launch traced here: 270 us
  waiting for transfers between devices  144 us (53%)
  matrix products  39.9 us (15%)
  blocking collectives  31.7 us (12%)
  other arithmetic  21.2 us (8%)
  local copies, waits for them, and re-layouts  19.3 us (7%)
  between operations  13.3 us (5%)
    reduce_scatter x1, waiting for transfers between devices, shards(): lax.psum_scatter(jnp.dot(attended, output_weight, preferred_element_type=...  50.1 us
    all_gather x1, waiting for transfers between devices, shards(): segment = lax.all_gather(packed, 'sp', axis=0, tiled=True)  46.9 us
    all_gather x1, waiting for transfers between devices, shards(): lax.all_gather(normed, 'tp', axis=0, tiled=True)  37.9 us
    psum x1, blocking collectives, shards(): summed = lax.psum(partial_mod, 'sp')  17.6 us
    all_gather x1, blocking collectives, shards(): mod_vectors = lax.all_gather(summed, 'tp', axis=2, tiled=True)  14.1 us
    dot_general x1, matrix products, shards(): jnp.dot(lax.all_gather(normed, 'tp', axis=0, tiled=True), projection, pre...  12.5 us
    dynamic_slice x4, local copies, waits for them, and re-layouts, shards(): lax.scan(one_block, state_now, stacked)[0]  11.9 us
    dot_general x3, matrix products, absorb(): jnp.einsum('mqhk,khd->mqhd', weights.astype(jnp.bfloat16), value_part, pr...  10.4 us
  transfers between devices with their start and end apart: 4, of which 4 were waited for; matrix products, arithmetic and copies ran while one was open for 12% of the time, Pallas kernels for 0%

commit v1 on v0

v1 whole, which is shorter than its diff:
```python
import functools

import jax
import jax.numpy as jnp
from jax import lax
from jax.experimental import pallas as pl
from jax.experimental.pallas import tpu as pltpu
from jax.sharding import PartitionSpec as P

GRID_W = 64
ROPE_BASE = 10000.0
EPSILON = 1e-05
LOG2E = 1.4426950408889634
ROWS = 16
VMEM_LIMIT = 62 * 1024 * 1024
MESH = pl.DeviceIdType.MESH


def remote(src, dst, send_sem, recv_sem, **where):
    return pltpu.make_async_remote_copy(
        src_ref=src,
        dst_ref=dst,
        send_sem=send_sem,
        recv_sem=recv_sem,
        device_id=where,
        device_id_type=MESH,
    )


def aligned(start, size, unit):
    return pl.ds(pl.multiple_of(start, unit), size)


def attend_kernel(
    sp_size,
    tp_size,
    latent,
    context,
    condition,
    context_condition,
    modulation,
    query_weight,
    key_weight,
    value_weight,
    cosine,
    sine,
    lambdas,
    lift,
    gain,
    attended,
    gate,
    tokens,
    context_tokens,
    normed,
    mod_weight,
    wq,
    wk,
    wv,
    keys_values,
    queries,
    mod_parts,
    mod_pieces,
    mod_rows,
    local_sem,
    tok_send,
    tok_recv,
    part_send,
    part_recv,
    piece_send,
    piece_recv,
    kv_send,
    kv_recv,
):
    s = lax.axis_index("sp")
    t = lax.axis_index("tp")
    z = lax.div(t, 2)
    c = lax.rem(t, 2)
    chips = tp_size // 2
    rows, width = latent.shape
    pair = 2 * rows
    block_tokens = tp_size * rows
    ctx_rows = context.shape[0]
    ctx_total = ctx_rows * sp_size
    local = query_weight.shape[1]
    heads = lambdas.shape[0]
    head = local // heads
    half = head // 2
    piece = modulation.shape[2]
    depth = modulation.shape[1]

    own_slot = tokens.at[aligned(t * rows, rows, ROWS)]
    locals_ = [
        pltpu.make_async_copy(src, dst, local_sem.at[i])
        for i, (src, dst) in enumerate(
            [
                (modulation, mod_weight),
                (latent, own_slot),
                (context, context_tokens),
                (key_weight, wk),
                (value_weight, wv),
                (query_weight, wq),
            ]
        )
    ]
    for copy in locals_:
        copy.start()

    barrier = pltpu.get_barrier_semaphore()
    for k in range(1, tp_size):
        pl.semaphore_signal(
            barrier, inc=1, device_id={"tp": lax.rem(t + k, tp_size)}, device_id_type=MESH
        )
    for k in range(1, sp_size):
        pl.semaphore_signal(
            barrier, inc=1, device_id={"sp": lax.rem(s + k, sp_size)}, device_id_type=MESH
        )
    pl.semaphore_wait(barrier, tp_size + sp_size - 2)

    def token_copy(kind, b, core, src=None):
        slot = 2 * b + core
        place = tokens.at[aligned(slot * rows, rows, ROWS)]
        to = (t + 2, t - 2, t + 1 - 2 * c)[kind]
        return remote(
            place if src is None else src,
            place,
            tok_send.at[kind, b],
            tok_recv.at[slot],
            tp=to,
        )

    @pl.when(z + 1 < chips)
    def _():
        token_copy(0, z, c, latent).start()

    @pl.when(z > 0)
    def _():
        token_copy(1, z, c, latent).start()

    token_copy(2, z, c, latent).start()

    def silu(ref):
        v = ref[:, aligned(s * depth, depth, 128)]
        return v / (1.0 + jnp.exp(-v))

    first = silu(condition)
    second = silu(context_condition)
    which = lax.broadcasted_iota(jnp.int32, (ROWS, depth), 0)
    vectors = jnp.where(
        which == 0, jnp.broadcast_to(first, (ROWS, depth)), jnp.broadcast_to(second, (ROWS, depth))
    ).astype(jnp.bfloat16)
    locals_[0].wait()
    for r in range(3):
        found = jnp.dot(vectors, mod_weight[r], preferred_element_type=jnp.float32)
        mod_parts[s, 2 * r : 2 * r + 2, :] = found[0:2]
    mod_parts[s, 6:8, :] = jnp.zeros((2, piece), jnp.float32)

    def part_copy(k, owner):
        return remote(
            mod_parts.at[owner],
            mod_parts.at[owner],
            part_send.at[k],
            part_recv.at[owner],
            sp=lax.rem(s + k, sp_size),
        )

    def piece_copy(k, owner):
        return remote(
            mod_pieces.at[owner],
            mod_pieces.at[owner],
            piece_send.at[k],
            piece_recv.at[owner],
            tp=lax.rem(t + k, tp_size),
        )

    for k in range(1, sp_size):
        part_copy(k, s).start()
    for k in range(1, sp_size):
        part_copy(k, lax.rem(s + k, sp_size)).wait_recv()
    total = mod_parts[0]
    for i in range(1, sp_size):
        total = total + mod_parts[i]
    mod_pieces[t] = total
    for k in range(1, tp_size):
        piece_copy(k, t).start()

    def forward(d):
        left = z - d
        right = z + d

        @pl.when(left >= 0)
        def _():
            token_copy(2, left, c).wait_recv()

            @pl.when(z + 1 < chips)
            def _():
                token_copy(0, left, c).start()

            token_copy(2, left, c).start()

        @pl.when(right < chips)
        def _():
            token_copy(2, right, c).wait_recv()

            @pl.when(z > 0)
            def _():
                token_copy(1, right, c).start()

            token_copy(2, right, c).start()

    forward(1)
    for k in range(1, tp_size):
        piece_copy(k, lax.rem(t + k, tp_size)).wait_recv()
    for i in range(tp_size):
        mod_rows[:, i * piece : (i + 1) * piece] = mod_pieces[i]
    gate[...] = mod_rows[4:5, :]

    def normalise(source, base, count, row):
        def group(i, carry):
            x = source[aligned(base + i * ROWS, ROWS, ROWS), :].astype(jnp.float32)
            x = x - jnp.sum(x, axis=1, keepdims=True) * (1.0 / width)
            spread = jnp.sum(x * x, axis=1, keepdims=True) * (1.0 / width)
            y = x * lax.rsqrt(spread + EPSILON)
            y = y * (1.0 + mod_rows[2 + row : 3 + row, :]) + mod_rows[row : row + 1, :]
            normed[aligned(i * ROWS, ROWS, ROWS), :] = y.astype(jnp.bfloat16)
            return carry

        lax.fori_loop(0, count // ROWS, group, 0)

    def kv_copy(k, owner, b, is_context):
        if is_context:
            place = keys_values.at[aligned(owner * ctx_rows, ctx_rows, ROWS)]
        else:
            place = keys_values.at[
                aligned(ctx_total + owner * block_tokens + b * pair, pair, ROWS)
            ]
        return remote(
            place, place, kv_send.at[k, b], kv_recv.at[owner, b], sp=lax.rem(s + k, sp_size)
        )

    locals_[1].wait()
    locals_[2].wait()
    normalise(context_tokens, 0, ctx_rows, 1)
    locals_[3].wait()
    locals_[4].wait()
    ctx_place = aligned(s * ctx_rows, ctx_rows, ROWS)
    keys_values[ctx_place, :local] = jnp.dot(
        normed[:ctx_rows, :], wk[...], preferred_element_type=jnp.float32
    ).astype(jnp.bfloat16)
    keys_values[ctx_place, local:] = jnp.dot(
        normed[:ctx_rows, :], wv[...], preferred_element_type=jnp.float32
    ).astype(jnp.bfloat16)
    for k in range(1, sp_size):
        kv_copy(k, s, chips, True).start()
    locals_[5].wait()

    quarter = half // 4
    lane = lax.broadcasted_iota(jnp.int32, (pair, half), 1)
    low = lax.rem(lane, 2 * quarter) < quarter

    def turn(raw, b):
        cos = cosine[aligned(b * pair, pair, ROWS), :]
        sin = sine[aligned(b * pair, pair, ROWS), :]
        parts = []
        for i in range(local // half):
            v = raw[:, i * half : (i + 1) * half].astype(jnp.bfloat16).astype(jnp.float32)
            other = jnp.where(low, pltpu.roll(v, half - quarter, 1), pltpu.roll(v, quarter, 1))
            parts.append((v * cos + other * sin).astype(jnp.bfloat16))
        return jnp.concatenate(parts, axis=1)

    def process(b):
        token_copy(2, b, 1 - c).wait_recv()
        normalise(tokens, b * pair, pair, 0)
        place = aligned(ctx_total + s * block_tokens + b * pair, pair, ROWS)
        x = normed[:pair, :]
        keys_values[place, :local] = turn(
            jnp.dot(x, wk[...], preferred_element_type=jnp.float32), b
        )
        keys_values[place, local:] = jnp.dot(
            x, wv[...], preferred_element_type=jnp.float32
        ).astype(jnp.bfloat16)
        for k in range(1, sp_size):
            kv_copy(k, s, b, False).start()
        queries[aligned(b * pair, pair, ROWS), :] = turn(
            jnp.dot(x, wq[...], preferred_element_type=jnp.float32), b
        )

    def step(j, carry):
        d = lax.div(j, 2)
        side = lax.rem(j, 2)

        @pl.when((side == 0) & (d >= 1) & (d + 1 < chips))
        def _():
            forward(d + 1)

        b = z - d + 2 * d * side

        @pl.when((b >= 0) & (b < chips) & (d + 1 > side))
        def _():
            process(b)

        return carry

    lax.fori_loop(0, 2 * chips, step, 0)

    for k in range(1, sp_size):
        owner = lax.rem(s + k, sp_size)
        kv_copy(k, owner, chips, True).wait_recv()
        for b in range(chips):
            kv_copy(k, owner, b, False).wait_recv()

    tile = min(256, block_tokens)
    key_total = keys_values.shape[0]
    factor = half ** (-0.5) * LOG2E
    on_context = lax.broadcasted_iota(jnp.int32, (1, key_total), 1) < ctx_total

    def attention(i, carry):
        place = aligned(i * tile, tile, ROWS)
        for h in range(heads):
            raised = jnp.where(on_context, lift[h] * LOG2E, 0.0)
            value = keys_values[:, local + h * head : local + (h + 1) * head]
            outs = []
            for m in range(2):
                at = h * head + m * half
                scores = lax.dot_general(
                    queries[place, at : at + half],
                    keys_values[:, at : at + half],
                    (((1,), (1,)), ((), ())),
                    preferred_element_type=jnp.float32,
                )
                scores = scores * factor + raised
                weights = jnp.exp2(scores - jnp.max(scores, axis=1, keepdims=True))
                sums = jnp.sum(weights, axis=1, keepdims=True)
                outs.append(
                    jnp.dot(
                        weights.astype(jnp.bfloat16), value, preferred_element_type=jnp.float32
                    )
                    / sums
                )
            diff = outs[0] - lambdas[h] * outs[1]
            mean = jnp.sum(diff * diff, axis=1, keepdims=True) * (1.0 / head)
            attended[place, h * head : (h + 1) * head] = (
                diff * lax.rsqrt(mean + EPSILON) * gain[...]
            ).astype(jnp.bfloat16)
        return carry

    lax.fori_loop(0, block_tokens // tile, attention, 0)

    for b in range(chips):

        @pl.when((b <= z) & (z + 1 < chips))
        def _():
            token_copy(0, b, c).wait_send()

        @pl.when((b >= z) & (z > 0))
        def _():
            token_copy(1, b, c).wait_send()

        token_copy(2, b, c).wait_send()
    for k in range(1, tp_size):
        piece_copy(k, t).wait_send()
    for k in range(1, sp_size):
        part_copy(k, s).wait_send()
        kv_copy(k, s, chips, True).wait_send()
        for b in range(chips):
            kv_copy(k, s, b, False).wait_send()


def output_kernel(
    tp_size,
    attended,
    output_weight,
    latent,
    gate,
    result,
    weight,
    own,
    pair_send,
    pair_recv,
    stage,
    from_left,
    from_right,
    local_sem,
    ps_sem,
    pr_sem,
    st_sem,
    left_sem,
    right_sem,
):
    t = lax.axis_index("tp")
    z = lax.div(t, 2)
    c = lax.rem(t, 2)
    chips = tp_size // 2
    rows, width = latent.shape
    chunk = min(1024, width)

    load = pltpu.make_async_copy(output_weight, weight, local_sem)
    load.start()
    barrier = pltpu.get_barrier_semaphore()

    @pl.when(z > 0)
    def _():
        pl.semaphore_signal(barrier, inc=1, device_id={"tp": t - 2}, device_id_type=MESH)

    @pl.when(z + 1 < chips)
    def _():
        pl.semaphore_signal(barrier, inc=1, device_id={"tp": t + 2}, device_id_type=MESH)

    pl.semaphore_signal(barrier, inc=1, device_id={"tp": t + 1 - 2 * c}, device_id_type=MESH)
    inner = (z > 0) & (z + 1 < chips)
    pl.semaphore_wait(barrier, jnp.where(inner, 3, 2) if chips > 1 else 1)

    load.wait()

    def pair_copy(b):
        return remote(
            pair_send.at[b], pair_recv.at[b], ps_sem.at[b], pr_sem.at[b], tp=t + 1 - 2 * c
        )

    def right_copy(b):
        return remote(stage.at[b], from_left.at[b], st_sem.at[b], left_sem.at[b], tp=t + 2)

    def left_copy(b):
        return remote(stage.at[b], from_right.at[b], st_sem.at[b], right_sem.at[b], tp=t - 2)

    def compute(b):
        other = attended[aligned((2 * b + 1 - c) * rows, rows, ROWS), :]
        mine = attended[aligned((2 * b + c) * rows, rows, ROWS), :]
        both = jnp.concatenate([other, mine], axis=0)
        for n in range(width // chunk):
            cols = slice(n * chunk, (n + 1) * chunk)
            found = jnp.dot(both, weight[:, cols], preferred_element_type=jnp.float32)
            pair_send[b, :, cols] = found[:rows].astype(jnp.bfloat16)
            own[b, :, cols] = found[rows:]
        pair_copy(b).start()

    def combine(b):
        pair_copy(b).wait_recv()

        @pl.when(b > z)
        def _():
            @pl.when(z > 0)
            def _():
                right_copy(b).wait_recv()
                stage[b] = (
                    own[b] + pair_recv[b].astype(jnp.float32) + from_left[b].astype(jnp.float32)
                ).astype(jnp.bfloat16)

            @pl.when(z == 0)
            def _():
                stage[b] = (own[b] + pair_recv[b].astype(jnp.float32)).astype(jnp.bfloat16)

            right_copy(b).start()

        @pl.when(b < z)
        def _():
            @pl.when(z + 1 < chips)
            def _():
                left_copy(b).wait_recv()
                stage[b] = (
                    own[b] + pair_recv[b].astype(jnp.float32) + from_right[b].astype(jnp.float32)
                ).astype(jnp.bfloat16)

            @pl.when(z + 1 == chips)
            def _():
                stage[b] = (own[b] + pair_recv[b].astype(jnp.float32)).astype(jnp.bfloat16)

            left_copy(b).start()

    def place_of(j):
        d = chips - 1 - lax.div(j, 2)
        side = lax.rem(j, 2)
        b = z - d + 2 * d * side
        return b, (b >= 0) & (b < chips) & (d + 1 > side)

    at_end = (z == 0) | (z + 1 == chips)

    def first_pass(j, carry):
        b, valid = place_of(j)

        @pl.when(valid)
        def _():
            compute(b)

            @pl.when(at_end & (b != z))
            def _():
                combine(b)

        return carry

    lax.fori_loop(0, 2 * chips, first_pass, 0)

    def second_pass(j, carry):
        b, valid = place_of(j)

        @pl.when(valid & jnp.logical_not(at_end) & (b != z))
        def _():
            combine(b)

        return carry

    lax.fori_loop(0, 2 * chips, second_pass, 0)

    pair_copy(z).wait_recv()
    own[z] = own[z] + pair_recv[z].astype(jnp.float32)

    @pl.when(z > 0)
    def _():
        right_copy(z).wait_recv()
        own[z] = own[z] + from_left[z].astype(jnp.float32)

    @pl.when(z + 1 < chips)
    def _():
        left_copy(z).wait_recv()
        own[z] = own[z] + from_right[z].astype(jnp.float32)

    result[...] = (latent[...].astype(jnp.float32) + gate[...] * own[z]).astype(jnp.bfloat16)

    for b in range(chips):
        pair_copy(b).wait_send()

        @pl.when(b > z)
        def _():
            right_copy(b).wait_send()

        @pl.when(b < z)
        def _():
            left_copy(b).wait_send()


def tables(places, half):
    quarter = half // 4
    inverse = ROPE_BASE ** (-jnp.arange(quarter, dtype=jnp.float32) / quarter)
    by_row = (places // GRID_W).astype(jnp.float32)[:, None] * inverse
    by_col = (places % GRID_W).astype(jnp.float32)[:, None] * inverse
    angles = jnp.concatenate([by_row, by_row, by_col, by_col], axis=1)
    sign = jnp.where(jnp.arange(half) % (2 * quarter) < quarter, -1.0, 1.0)
    return jnp.cos(angles), jnp.sin(angles) * sign


def shards(
    sp_size,
    tp_size,
    latent,
    context,
    condition,
    context_condition,
    modulation,
    query_weight,
    key_weight,
    value_weight,
    lambdas,
    context_lift,
    head_gain,
    output_weight,
):
    rows, width = latent.shape
    chips = tp_size // 2
    local = query_weight.shape[1]
    half = local // lambdas.shape[0] // 2
    block_tokens = rows * tp_size
    ctx_rows = context.shape[0]
    piece = modulation.shape[2]
    places = lax.axis_index("sp") * block_tokens + jnp.arange(block_tokens, dtype=jnp.int32)
    cosine, sine = tables(places, half)
    vmem = pl.BlockSpec(memory_space=pltpu.VMEM)
    smem = pl.BlockSpec(memory_space=pltpu.SMEM)
    anywhere = pl.BlockSpec(memory_space=pl.ANY)
    bf16, f32 = jnp.bfloat16, jnp.float32
    dma = pltpu.SemaphoreType.DMA
    attended, gate = pl.pallas_call(
        functools.partial(attend_kernel, sp_size, tp_size),
        out_shape=(
            jax.ShapeDtypeStruct((block_tokens, local), bf16),
            jax.ShapeDtypeStruct((1, width), f32),
        ),
        in_specs=[anywhere] * 2 + [vmem] * 2 + [anywhere] * 4 + [vmem] * 2 + [smem] * 2 + [vmem],
        out_specs=(vmem, vmem),
        scratch_shapes=[
            pltpu.VMEM((block_tokens, width), bf16),
            pltpu.VMEM(context.shape, bf16),
            pltpu.VMEM((max(2 * rows, ctx_rows), width), bf16),
            pltpu.VMEM(modulation.shape, bf16),
            pltpu.VMEM((width, local), bf16),
            pltpu.VMEM((width, local), bf16),
            pltpu.VMEM((width, local), bf16),
            pltpu.VMEM((sp_size * (ctx_rows + block_tokens), 2 * local), bf16),
            pltpu.VMEM((block_tokens, local), bf16),
            pltpu.VMEM((sp_size, 8, piece), f32),
            pltpu.VMEM((tp_size, 8, piece), f32),
            pltpu.VMEM((8, width), f32),
            dma((6,)),
            dma((3, chips)),
            dma((tp_size,)),
            dma((sp_size,)),
            dma((sp_size,)),
            dma((tp_size,)),
            dma((tp_size,)),
            dma((sp_size, chips + 1)),
            dma((sp_size, chips + 1)),
        ],
        compiler_params=pltpu.CompilerParams(
            collective_id=0, has_side_effects=True, vmem_limit_bytes=VMEM_LIMIT
        ),
        name="attend",
    )(
        latent,
        context,
        condition.reshape(1, -1),
        context_condition.reshape(1, -1),
        modulation,
        query_weight,
        key_weight,
        value_weight,
        cosine,
        sine,
        lambdas,
        context_lift,
        head_gain.reshape(1, -1),
    )
    blocks = (chips, rows, width)
    return pl.pallas_call(
        functools.partial(output_kernel, tp_size),
        out_shape=jax.ShapeDtypeStruct((rows, width), bf16),
        in_specs=[vmem, anywhere, vmem, vmem],
        out_specs=vmem,
        scratch_shapes=[
            pltpu.VMEM(output_weight.shape, bf16),
            pltpu.VMEM(blocks, f32),
            pltpu.VMEM(blocks, bf16),
            pltpu.VMEM(blocks, bf16),
            pltpu.VMEM(blocks, bf16),
            pltpu.VMEM(blocks, bf16),
            pltpu.VMEM(blocks, bf16),
            dma(()),
            dma((chips,)),
            dma((chips,)),
            dma((chips,)),
            dma((chips,)),
            dma((chips,)),
        ],
        compiler_params=pltpu.CompilerParams(
            collective_id=1, has_side_effects=True, vmem_limit_bytes=VMEM_LIMIT
        ),
        name="output",
    )(attended, output_weight, latent, gate)


def solution(mesh):
    in_specs = (
        P(("sp", "tp"), None),
        P("sp", None),
        P(),
        P(),
        P(None, "sp", "tp"),
        P(None, "tp"),
        P(None, "tp"),
        P(None, "tp"),
        P("tp"),
        P("tp"),
        P(),
        P("tp", None),
    )
    out_specs = P(("sp", "tp"), None)
    body = functools.partial(shards, mesh.shape["sp"], mesh.shape["tp"])
    return jax.shard_map(body, mesh=mesh, in_specs=in_specs, out_specs=out_specs, check_vma=False)
```

time: 271 us -> 147 us (0.54)
  waiting for transfers between devices: 144 us -> 0 us
  Pallas kernels: 0 us -> 143 us
  matrix products: 39.9 us -> 0 us
  blocking collectives: 31.7 us -> 0 us
  other arithmetic: 21.2 us -> 2.09 us
  local copies, waits for them, and re-layouts: 19.3 us -> 1.87 us
  between operations: 13.3 us -> 0.03 us
    pallas_call x0 -> x2, Pallas kernels: none -> 143 us  [the longest x1 94.8 us: shards(): pl.pallas_call(functools.partial(attend_kernel, sp_size, tp_size), out_sh...]
    all_gather x3 -> x0, waiting for transfers between devices: 93.9 us -> none  [the longest x1 46.9 us: shards(): segment = lax.all_gather(packed, 'sp', axis=0, tiled=True)]
    reduce_scatter x1 -> x0, waiting for transfers between devices: 50.1 us -> none  [shards(): lax.psum_scatter(jnp.dot(attended, output_weight, preferred_element_type=...]
    dot_general x10 -> x0, matrix products: 39.9 us -> none  [the longest x1 12.5 us: shards(): jnp.dot(lax.all_gather(normed, 'tp', axis=0, tiled=True), projection, pre...]
    psum x1 -> x0, blocking collectives: 17.6 us -> none  [shards(): summed = lax.psum(partial_mod, 'sp')]
    all_gather x1 -> x0, blocking collectives: 14.1 us -> none  [shards(): mod_vectors = lax.all_gather(summed, 'tp', axis=2, tiled=True)]
    dynamic_slice x4 -> x0, local copies, waits for them, and re-layouts: 11.9 us -> none  [shards(): lax.scan(one_block, state_now, stacked)[0]]
    convert_element_type x7 -> x1, other arithmetic: 8.77 us -> 0.01 us  [tables(): by_row = (places // GRID_W).astype(jnp.float32)[:, None] * inverse]
  transfers between devices with their start and end apart: 4 -> 0, of which waited for: 4 -> 0; matrix products, arithmetic and copies ran while one was open for 12% -> 0% of each run, Pallas kernels for 0% -> 0%
where the time goes in v1:
time: 147 us
  Pallas kernels  143 us (97%)
  other arithmetic  2.09 us (1%)
  local copies, waits for them, and re-layouts  1.87 us (1%)
    pallas_call x1, Pallas kernels, shards(): pl.pallas_call(functools.partial(attend_kernel, sp_size, tp_size), out_sh...  94.8 us
    pallas_call x1, Pallas kernels, shards(): pl.pallas_call(functools.partial(output_kernel, tp_size), out_shape=jax.S...  47.8 us

profile of v1, /device:TPU:0, one launch (start us, length us, event | category | flops | bytes accessed | tf_op | source)
XLA Modules:
  0.0 146.6 jit_solution(14083810605333987050)
XLA Ops:
  0.0 0.2 broadcast_multiply_fusion.1
  0.2 1.9 %sine_multiply_fusion = (f32[512,128]{1,0:T(8,128)}, f32[512,128]{1,0:T(8,128)}) fusion(f32[128]{0:T(128)S(1)} %compare_select_fusion, f32[512,32]{1,0:T(8,128)S(1)} %get-tuple-element.12, f32[512,32]{1,0:T(8,128)S(1)} %get-tuple-element.11), kind=kLoop, calls=%fused_computation.1 | loop fusion | flops 262144 | bytes 655872 | tf_op jit(solution)/shard_map/mul | solution.py:537
  2.1 94.8 %attend.1 = (bf16[512,512]{1,0:T(8,128)(2,1)}, f32[1,4096]{1,0:T(1,128)}) custom-call(bf16[64,4096]{1,0:T(8,128)(2,1)} %latent.3, bf16[128,4096]{1,0:T(8,128)(2,1)} %context.1, f32[1,4096]{1,0:T(1,128)} %bitcast.3, f32[1,4096]{1,0:T(1,128)} %bitcast.4, bf16[3,1024,512]{2,1,0:T(8,128)(2,1)} %modulation.1, bf16[4096,512]{1,0:T(8,128)(2,1)} %query_weight.1, ...), custom_call_target="tpu_custom_call" | custom-call | tf_op jit(solution)/shard_map/attend/pallas_call | solution.py:570
  96.9 47.8 %output.1 = bf16[64,4096]{1,0:T(8,128)(2,1)} custom-call(bf16[512,512]{1,0:T(8,128)(2,1)} %get-tuple-element.7.attended, bf16[512,4096]{1,0:T(8,128)(2,1)} %output_weight.1, bf16[64,4096]{1,0:T(8,128)(2,1)} %latent.3, f32[1,4096]{1,0:T(1,128)} %get-tuple-element.8.gate), custom_call_target="tpu_custom_call" | custom-call | tf_op jit(solution)/shard_map/output/pallas_call | solution.py:621
  144.8 1.9 %copy.14 = bf16[64,4096]{1,0:T(8,128)(2,1)} copy(bf16[64,4096]{1,0:T(8,128)(2,1)} %output.1) | data formatting | bytes 1048576
  (3 shorter events, 0.0 us)

commit v2 on v1

--- a/solution.py
+++ b/solution.py
@@ -58,6 +58,9 @@
     wv,
     keys_values,
     queries,
+    kv_stage,
+    q_stage,
+    out_stage,
     mod_parts,
     mod_pieces,
     mod_rows,
@@ -70,6 +73,10 @@
     piece_recv,
     kv_send,
     kv_recv,
+    q_send,
+    q_recv,
+    out_send,
+    out_recv,
 ):
     s = lax.axis_index("sp")
     t = lax.axis_index("tp")
@@ -226,31 +233,74 @@
 
         lax.fori_loop(0, count // ROWS, group, 0)
 
+    my_head = lax.rem(s, heads)
+
+    def mate(k):
+        return lax.rem(my_head + k, heads)
+
+    def kv_place(owner, b, is_context):
+        if is_context:
+            return aligned(owner * ctx_rows, ctx_rows, ROWS)
+        return aligned(ctx_total + owner * block_tokens + b * pair, pair, ROWS)
+
+    def stage_place(b, is_context):
+        if is_context:
+            return aligned(block_tokens, ctx_rows, ROWS)
+        return aligned(b * pair, pair, ROWS)
+
     def kv_copy(k, owner, b, is_context):
-        if is_context:
-            place = keys_values.at[aligned(owner * ctx_rows, ctx_rows, ROWS)]
-        else:
-            place = keys_values.at[
-                aligned(ctx_total + owner * block_tokens + b * pair, pair, ROWS)
-            ]
+        to = lax.rem(s + k, sp_size)
         return remote(
-            place, place, kv_send.at[k, b], kv_recv.at[owner, b], sp=lax.rem(s + k, sp_size)
-        )
+            kv_stage.at[lax.rem(to, heads), stage_place(b, is_context)],
+            keys_values.at[kv_place(owner, b, is_context)],
+            kv_send.at[k, b],
+            kv_recv.at[owner, b],
+            sp=to,
+        )
+
+    def q_copy(k, slot, b):
+        place = aligned(b * pair, pair, ROWS)
+        return remote(
+            q_stage.at[mate(k), place],
+            queries.at[slot, place],
+            q_send.at[k, b],
+            q_recv.at[slot, b],
+            sp=s - my_head + mate(k),
+        )
+
+    def out_copy(k, head_index):
+        return remote(
+            out_stage.at[mate(k)],
+            attended.at[head_index],
+            out_send.at[k],
+            out_recv.at[head_index],
+            sp=s - my_head + mate(k),
+        )
+
+    def hand_out(keys, values, b, is_context):
+        place = stage_place(b, is_context)
+        for g in range(heads):
+            kv_stage[g, place, :head] = keys[:, g * head : (g + 1) * head]
+            kv_stage[g, place, head:] = values[:, g * head : (g + 1) * head]
+        for k in range(1, sp_size):
+            kv_copy(k, s, b, is_context).start()
+        keys_values[kv_place(s, b, is_context), :] = kv_stage[my_head, place, :]
 
     locals_[1].wait()
     locals_[2].wait()
     normalise(context_tokens, 0, ctx_rows, 1)
     locals_[3].wait()
     locals_[4].wait()
-    ctx_place = aligned(s * ctx_rows, ctx_rows, ROWS)
-    keys_values[ctx_place, :local] = jnp.dot(
-        normed[:ctx_rows, :], wk[...], preferred_element_type=jnp.float32
-    ).astype(jnp.bfloat16)
-    keys_values[ctx_place, local:] = jnp.dot(
-        normed[:ctx_rows, :], wv[...], preferred_element_type=jnp.float32
-    ).astype(jnp.bfloat16)
-    for k in range(1, sp_size):
-        kv_copy(k, s, chips, True).start()
+    hand_out(
+        jnp.dot(normed[:ctx_rows, :], wk[...], preferred_element_type=jnp.float32).astype(
+            jnp.bfloat16
+        ),
+        jnp.dot(normed[:ctx_rows, :], wv[...], preferred_element_type=jnp.float32).astype(
+            jnp.bfloat16
+        ),
+        chips,
+        True,
+    )
     locals_[5].wait()
 
     quarter = half // 4
@@ -270,19 +320,20 @@
     def process(b):
         token_copy(2, b, 1 - c).wait_recv()
         normalise(tokens, b * pair, pair, 0)
-        place = aligned(ctx_total + s * block_tokens + b * pair, pair, ROWS)
         x = normed[:pair, :]
-        keys_values[place, :local] = turn(
-            jnp.dot(x, wk[...], preferred_element_type=jnp.float32), b
-        )
-        keys_values[place, local:] = jnp.dot(
-            x, wv[...], preferred_element_type=jnp.float32
-        ).astype(jnp.bfloat16)
-        for k in range(1, sp_size):
-            kv_copy(k, s, b, False).start()
-        queries[aligned(b * pair, pair, ROWS), :] = turn(
-            jnp.dot(x, wq[...], preferred_element_type=jnp.float32), b
-        )
+        hand_out(
+            turn(jnp.dot(x, wk[...], preferred_element_type=jnp.float32), b),
+            jnp.dot(x, wv[...], preferred_element_type=jnp.float32).astype(jnp.bfloat16),
+            b,
+            False,
+        )
+        turned = turn(jnp.dot(x, wq[...], preferred_element_type=jnp.float32), b)
+        place = aligned(b * pair, pair, ROWS)
+        for g in range(heads):
+            q_stage[g, place, :] = turned[:, g * head : (g + 1) * head]
+        for k in range(1, heads):
+            q_copy(k, my_head, b).start()
+        queries[my_head, place, :] = q_stage[my_head, place, :]
 
     def step(j, carry):
         d = lax.div(j, 2)
@@ -307,43 +358,56 @@
         kv_copy(k, owner, chips, True).wait_recv()
         for b in range(chips):
             kv_copy(k, owner, b, False).wait_recv()
+    for k in range(1, heads):
+        for b in range(chips):
+            q_copy(k, mate(k), b).wait_recv()
 
     tile = min(256, block_tokens)
     key_total = keys_values.shape[0]
     factor = half ** (-0.5) * LOG2E
     on_context = lax.broadcasted_iota(jnp.int32, (1, key_total), 1) < ctx_total
 
-    def attention(i, carry):
+    raised = jnp.where(on_context, lift[my_head] * LOG2E, 0.0)
+    weight_of_second = lambdas[my_head]
+
+    def attention(i, slot):
         place = aligned(i * tile, tile, ROWS)
-        for h in range(heads):
-            raised = jnp.where(on_context, lift[h] * LOG2E, 0.0)
-            value = keys_values[:, local + h * head : local + (h + 1) * head]
-            outs = []
-            for m in range(2):
-                at = h * head + m * half
-                scores = lax.dot_general(
-                    queries[place, at : at + half],
-                    keys_values[:, at : at + half],
-                    (((1,), (1,)), ((), ())),
+        outs = []
+        for m in range(2):
+            scores = lax.dot_general(
+                queries[slot, place, m * half : (m + 1) * half],
+                keys_values[:, m * half : (m + 1) * half],
+                (((1,), (1,)), ((), ())),
+                preferred_element_type=jnp.float32,
+            )
+            scores = scores * factor + raised
+            weights = jnp.exp2(scores - jnp.max(scores, axis=1, keepdims=True))
+            sums = jnp.sum(weights, axis=1, keepdims=True)
+            outs.append(
+                jnp.dot(
+                    weights.astype(jnp.bfloat16),
+                    keys_values[:, head:],
                     preferred_element_type=jnp.float32,
                 )
-                scores = scores * factor + raised
-                weights = jnp.exp2(scores - jnp.max(scores, axis=1, keepdims=True))
-                sums = jnp.sum(weights, axis=1, keepdims=True)
-                outs.append(
-                    jnp.dot(
-                        weights.astype(jnp.bfloat16), value, preferred_element_type=jnp.float32
-                    )
-                    / sums
-                )
-            diff = outs[0] - lambdas[h] * outs[1]
-            mean = jnp.sum(diff * diff, axis=1, keepdims=True) * (1.0 / head)
-            attended[place, h * head : (h + 1) * head] = (
-                diff * lax.rsqrt(mean + EPSILON) * gain[...]
-            ).astype(jnp.bfloat16)
-        return carry
-
-    lax.fori_loop(0, block_tokens // tile, attention, 0)
+                / sums
+            )
+        diff = outs[0] - weight_of_second * outs[1]
+        mean = jnp.sum(diff * diff, axis=1, keepdims=True) * (1.0 / head)
+        out_stage[slot, place, :] = (diff * lax.rsqrt(mean + EPSILON) * gain[...]).astype(
+            jnp.bfloat16
+        )
+        return slot
+
+    for k in range(1, heads + 1):
+        lax.fori_loop(0, block_tokens // tile, attention, mate(k))
+        if k < heads:
+            out_copy(k, my_head).start()
+    attended[my_head] = out_stage[my_head]
+    for k in range(1, heads):
+        out_copy(k, mate(k)).wait_recv()
+        out_copy(k, my_head).wait_send()
+        for b in range(chips):
+            q_copy(k, my_head, b).wait_send()
 
     for b in range(chips):
 
@@ -423,9 +487,15 @@
         return remote(stage.at[b], from_right.at[b], st_sem.at[b], right_sem.at[b], tp=t - 2)
 
     def compute(b):
-        other = attended[aligned((2 * b + 1 - c) * rows, rows, ROWS), :]
-        mine = attended[aligned((2 * b + c) * rows, rows, ROWS), :]
-        both = jnp.concatenate([other, mine], axis=0)
+        other = aligned((2 * b + 1 - c) * rows, rows, ROWS)
+        mine = aligned((2 * b + c) * rows, rows, ROWS)
+        both = jnp.concatenate(
+            [
+                jnp.concatenate([attended[g, part, :] for g in range(attended.shape[0])], axis=1)
+                for part in (other, mine)
+            ],
+            axis=0,
+        )
         for n in range(width // chunk):
             cols = slice(n * chunk, (n + 1) * chunk)
             found = jnp.dot(both, weight[:, cols], preferred_element_type=jnp.float32)
@@ -556,7 +626,9 @@
     rows, width = latent.shape
     chips = tp_size // 2
     local = query_weight.shape[1]
-    half = local // lambdas.shape[0] // 2
+    heads = lambdas.shape[0]
+    head = local // heads
+    half = head // 2
     block_tokens = rows * tp_size
     ctx_rows = context.shape[0]
     piece = modulation.shape[2]
@@ -570,7 +642,7 @@
     attended, gate = pl.pallas_call(
         functools.partial(attend_kernel, sp_size, tp_size),
         out_shape=(
-            jax.ShapeDtypeStruct((block_tokens, local), bf16),
+            jax.ShapeDtypeStruct((heads, block_tokens, head), bf16),
             jax.ShapeDtypeStruct((1, width), f32),
         ),
         in_specs=[anywhere] * 2 + [vmem] * 2 + [anywhere] * 4 + [vmem] * 2 + [smem] * 2 + [vmem],
@@ -583,8 +655,11 @@
             pltpu.VMEM((width, local), bf16),
             pltpu.VMEM((width, local), bf16),
             pltpu.VMEM((width, local), bf16),
-            pltpu.VMEM((sp_size * (ctx_rows + block_tokens), 2 * local), bf16),
-            pltpu.VMEM((block_tokens, local), bf16),
+            pltpu.VMEM((sp_size * (ctx_rows + block_tokens), 2 * head), bf16),
+            pltpu.VMEM((heads, block_tokens, head), bf16),
+            pltpu.VMEM((heads, block_tokens + ctx_rows, 2 * head), bf16),
+            pltpu.VMEM((heads, block_tokens, head), bf16),
+            pltpu.VMEM((heads, block_tokens, head), bf16),
             pltpu.VMEM((sp_size, 8, piece), f32),
             pltpu.VMEM((tp_size, 8, piece), f32),
             pltpu.VMEM((8, width), f32),
@@ -597,6 +672,10 @@
             dma((tp_size,)),
             dma((sp_size, chips + 1)),
             dma((sp_size, chips + 1)),
+            dma((heads, chips)),
+            dma((heads, chips)),
+            dma((heads,)),
+            dma((heads,)),
         ],
         compiler_params=pltpu.CompilerParams(
             collective_id=0, has_side_effects=True, vmem_limit_bytes=VMEM_LIMIT

time: 147 us -> 125 us (0.85)
  Pallas kernels: 143 us -> 120 us
    pallas_call x1, Pallas kernels: 94.8 us -> 77.1 us  [shards(): pl.pallas_call(functools.partial(attend_kernel, sp_size, tp_size), out_sh...]
    pallas_call x1, Pallas kernels: 47.8 us -> 43.3 us  [shards(): pl.pallas_call(functools.partial(output_kernel, tp_size), out_shape=jax.S...]
where the time goes in v2:
time: 125 us; the launch traced here: 124 us
  Pallas kernels  120 us (96%)
  other arithmetic  2.09 us (2%)
  local copies, waits for them, and re-layouts  1.87 us (1%)
    pallas_call x1, Pallas kernels, shards(): pl.pallas_call(functools.partial(attend_kernel, sp_size, tp_size), out_sh...  77.1 us
    pallas_call x1, Pallas kernels, shards(): pl.pallas_call(functools.partial(output_kernel, tp_size), out_shape=jax.S...  43.3 us

profile of v2, /device:TPU:0, one launch (start us, length us, event | category | flops | bytes accessed | tf_op | source)
XLA Modules:
  0.0 124.4 jit_solution(9414968370676168739)
XLA Ops:
  0.0 0.2 broadcast_multiply_fusion.1
  0.2 1.9 %sine_multiply_fusion = (f32[512,128]{1,0:T(8,128)}, f32[512,128]{1,0:T(8,128)}) fusion(f32[128]{0:T(128)S(1)} %compare_select_fusion, f32[512,32]{1,0:T(8,128)S(1)} %get-tuple-element.12, f32[512,32]{1,0:T(8,128)S(1)} %get-tuple-element.11), kind=kLoop, calls=%fused_computation.1 | loop fusion | flops 262144 | bytes 655872 | tf_op jit(solution)/shard_map/mul | solution.py:607
  2.1 77.1 %attend.1 = (bf16[2,512,256]{2,1,0:T(8,128)(2,1)}, f32[1,4096]{1,0:T(1,128)}) custom-call(bf16[64,4096]{1,0:T(8,128)(2,1)} %latent.3, bf16[128,4096]{1,0:T(8,128)(2,1)} %context.1, f32[1,4096]{1,0:T(1,128)} %bitcast.3, f32[1,4096]{1,0:T(1,128)} %bitcast.4, bf16[3,1024,512]{2,1,0:T(8,128)(2,1)} %modulation.1, bf16[4096,512]{1,0:T(8,128)(2,1)} %query_weight.1, ...), custom_call_target="tpu_custom_call" | custom-call | tf_op jit(solution)/shard_map/attend/pallas_call | solution.py:642
  79.3 43.3 %output.1 = bf16[64,4096]{1,0:T(8,128)(2,1)} custom-call(bf16[2,512,256]{2,1,0:T(8,128)(2,1)} %get-tuple-element.7.attended, bf16[512,4096]{1,0:T(8,128)(2,1)} %output_weight.1, bf16[64,4096]{1,0:T(8,128)(2,1)} %latent.3, f32[1,4096]{1,0:T(1,128)} %get-tuple-element.8.gate), custom_call_target="tpu_custom_call" | custom-call | tf_op jit(solution)/shard_map/output/pallas_call | solution.py:700
  122.5 1.9 %copy.14 = bf16[64,4096]{1,0:T(8,128)(2,1)} copy(bf16[64,4096]{1,0:T(8,128)(2,1)} %output.1) | data formatting | bytes 1048576
  (3 shorter events, 0.0 us)

commit v3 on v2

--- a/solution.py
+++ b/solution.py
@@ -123,27 +123,31 @@
         )
     pl.semaphore_wait(barrier, tp_size + sp_size - 2)
 
-    def token_copy(kind, b, core, src=None):
+    part_rows = rows // 2
+
+    def token_copy(kind, b, core, part, own=False):
         slot = 2 * b + core
-        place = tokens.at[aligned(slot * rows, rows, ROWS)]
+        place = tokens.at[aligned(slot * rows + part * part_rows, part_rows, ROWS)]
         to = (t + 2, t - 2, t + 1 - 2 * c)[kind]
         return remote(
-            place if src is None else src,
+            latent.at[part * part_rows : (part + 1) * part_rows] if own else place,
             place,
-            tok_send.at[kind, b],
-            tok_recv.at[slot],
+            tok_send.at[kind, 2 * b + part],
+            tok_recv.at[2 * slot + part],
             tp=to,
         )
 
-    @pl.when(z + 1 < chips)
-    def _():
-        token_copy(0, z, c, latent).start()
-
-    @pl.when(z > 0)
-    def _():
-        token_copy(1, z, c, latent).start()
-
-    token_copy(2, z, c, latent).start()
+    for part in range(2):
+
+        @pl.when(z + 1 < chips)
+        def _():
+            token_copy(0, z, c, part, True).start()
+
+        @pl.when(z > 0)
+        def _():
+            token_copy(1, z, c, part, True).start()
+
+        token_copy(2, z, c, part, True).start()
 
     def silu(ref):
         v = ref[:, aligned(s * depth, depth, 128)]
@@ -194,25 +198,27 @@
         left = z - d
         right = z + d
 
-        @pl.when(left >= 0)
-        def _():
-            token_copy(2, left, c).wait_recv()
-
-            @pl.when(z + 1 < chips)
-            def _():
-                token_copy(0, left, c).start()
-
-            token_copy(2, left, c).start()
-
-        @pl.when(right < chips)
-        def _():
-            token_copy(2, right, c).wait_recv()
-
-            @pl.when(z > 0)
-            def _():
-                token_copy(1, right, c).start()
-
-            token_copy(2, right, c).start()
+        for part in range(2):
+
+            @pl.when(left >= 0)
+            def _():
+                token_copy(2, left, c, part).wait_recv()
+
+                @pl.when(z + 1 < chips)
+                def _():
+                    token_copy(0, left, c, part).start()
+
+                token_copy(2, left, c, part).start()
+
+            @pl.when(right < chips)
+            def _():
+                token_copy(2, right, c, part).wait_recv()
+
+                @pl.when(z > 0)
+                def _():
+                    token_copy(1, right, c, part).start()
+
+                token_copy(2, right, c, part).start()
 
     forward(1)
     for k in range(1, tp_size):
@@ -287,21 +293,8 @@
         keys_values[kv_place(s, b, is_context), :] = kv_stage[my_head, place, :]
 
     locals_[1].wait()
-    locals_[2].wait()
-    normalise(context_tokens, 0, ctx_rows, 1)
-    locals_[3].wait()
-    locals_[4].wait()
-    hand_out(
-        jnp.dot(normed[:ctx_rows, :], wk[...], preferred_element_type=jnp.float32).astype(
-            jnp.bfloat16
-        ),
-        jnp.dot(normed[:ctx_rows, :], wv[...], preferred_element_type=jnp.float32).astype(
-            jnp.bfloat16
-        ),
-        chips,
-        True,
-    )
-    locals_[5].wait()
+    for i in (3, 4, 5):
+        locals_[i].wait()
 
     quarter = half // 4
     lane = lax.broadcasted_iota(jnp.int32, (pair, half), 1)
@@ -318,7 +311,8 @@
         return jnp.concatenate(parts, axis=1)
 
     def process(b):
-        token_copy(2, b, 1 - c).wait_recv()
+        for part in range(2):
+            token_copy(2, b, 1 - c, part).wait_recv()
         normalise(tokens, b * pair, pair, 0)
         x = normed[:pair, :]
         hand_out(
@@ -335,11 +329,31 @@
             q_copy(k, my_head, b).start()
         queries[my_head, place, :] = q_stage[my_head, place, :]
 
+    def process_context():
+        locals_[2].wait()
+        normalise(context_tokens, 0, ctx_rows, 1)
+        hand_out(
+            jnp.dot(normed[:ctx_rows, :], wk[...], preferred_element_type=jnp.float32).astype(
+                jnp.bfloat16
+            ),
+            jnp.dot(normed[:ctx_rows, :], wv[...], preferred_element_type=jnp.float32).astype(
+                jnp.bfloat16
+            ),
+            chips,
+            True,
+        )
+
     def step(j, carry):
         d = lax.div(j, 2)
         side = lax.rem(j, 2)
 
-        @pl.when((side == 0) & (d >= 1) & (d + 1 < chips))
+        @pl.when(j == 1)
+        def _():
+            if chips > 2:
+                forward(2)
+            process_context()
+
+        @pl.when((side == 0) & (d >= 2) & (d + 1 < chips))
         def _():
             forward(d + 1)
 
@@ -410,16 +424,17 @@
             q_copy(k, my_head, b).wait_send()
 
     for b in range(chips):
-
-        @pl.when((b <= z) & (z + 1 < chips))
-        def _():
-            token_copy(0, b, c).wait_send()
-
-        @pl.when((b >= z) & (z > 0))
-        def _():
-            token_copy(1, b, c).wait_send()
-
-        token_copy(2, b, c).wait_send()
+        for part in range(2):
+
+            @pl.when((b <= z) & (z + 1 < chips))
+            def _():
+                token_copy(0, b, c, part).wait_send()
+
+            @pl.when((b >= z) & (z > 0))
+            def _():
+                token_copy(1, b, c, part).wait_send()
+
+            token_copy(2, b, c, part).wait_send()
     for k in range(1, tp_size):
         piece_copy(k, t).wait_send()
     for k in range(1, sp_size):
@@ -455,7 +470,8 @@
     c = lax.rem(t, 2)
     chips = tp_size // 2
     rows, width = latent.shape
-    chunk = min(1024, width)
+    span = width // 2
+    chunk = min(1024, span)
 
     load = pltpu.make_async_copy(output_weight, weight, local_sem)
     load.start()
@@ -486,7 +502,8 @@
     def left_copy(b):
         return remote(stage.at[b], from_right.at[b], st_sem.at[b], right_sem.at[b], tp=t - 2)
 
-    def compute(b):
+    def compute(b, part):
+        u = 2 * b + part
         other = aligned((2 * b + 1 - c) * rows, rows, ROWS)
         mine = aligned((2 * b + c) * rows, rows, ROWS)
         both = jnp.concatenate(
@@ -496,105 +513,115 @@
             ],
             axis=0,
         )
-        for n in range(width // chunk):
+        for n in range(span // chunk):
             cols = slice(n * chunk, (n + 1) * chunk)
-            found = jnp.dot(both, weight[:, cols], preferred_element_type=jnp.float32)
-            pair_send[b, :, cols] = found[:rows].astype(jnp.bfloat16)
-            own[b, :, cols] = found[rows:]
-        pair_copy(b).start()
-
-    def combine(b):
-        pair_copy(b).wait_recv()
+            found = jnp.dot(
+                both,
+                weight[:, aligned(part * span + n * chunk, chunk, 128)],
+                preferred_element_type=jnp.float32,
+            )
+            pair_send[u, :, cols] = found[:rows].astype(jnp.bfloat16)
+            own[u, :, cols] = found[rows:]
+        pair_copy(u).start()
+
+    def combine(b, part):
+        u = 2 * b + part
+        pair_copy(u).wait_recv()
 
         @pl.when(b > z)
         def _():
             @pl.when(z > 0)
             def _():
-                right_copy(b).wait_recv()
-                stage[b] = (
-                    own[b] + pair_recv[b].astype(jnp.float32) + from_left[b].astype(jnp.float32)
+                right_copy(u).wait_recv()
+                stage[u] = (
+                    own[u] + pair_recv[u].astype(jnp.float32) + from_left[u].astype(jnp.float32)
                 ).astype(jnp.bfloat16)
 
             @pl.when(z == 0)
             def _():
-                stage[b] = (own[b] + pair_recv[b].astype(jnp.float32)).astype(jnp.bfloat16)
-
-            right_copy(b).start()
+                stage[u] = (own[u] + pair_recv[u].astype(jnp.float32)).astype(jnp.bfloat16)
+
+            right_copy(u).start()
 
         @pl.when(b < z)
         def _():
             @pl.when(z + 1 < chips)
             def _():
-                left_copy(b).wait_recv()
-                stage[b] = (
-                    own[b] + pair_recv[b].astype(jnp.float32) + from_right[b].astype(jnp.float32)
+                left_copy(u).wait_recv()
+                stage[u] = (
+                    own[u] + pair_recv[u].astype(jnp.float32) + from_right[u].astype(jnp.float32)
                 ).astype(jnp.bfloat16)
 
             @pl.when(z + 1 == chips)
             def _():
-                stage[b] = (own[b] + pair_recv[b].astype(jnp.float32)).astype(jnp.bfloat16)
-
-            left_copy(b).start()
+                stage[u] = (own[u] + pair_recv[u].astype(jnp.float32)).astype(jnp.bfloat16)
+
+            left_copy(u).start()
 
     def place_of(j):
-        d = chips - 1 - lax.div(j, 2)
-        side = lax.rem(j, 2)
+        d = chips - 1 - lax.div(j, 4)
+        side = lax.rem(lax.div(j, 2), 2)
         b = z - d + 2 * d * side
-        return b, (b >= 0) & (b < chips) & (d + 1 > side)
+        return b, lax.rem(j, 2), (b >= 0) & (b < chips) & (d + 1 > side)
 
     at_end = (z == 0) | (z + 1 == chips)
 
     def first_pass(j, carry):
-        b, valid = place_of(j)
+        b, part, valid = place_of(j)
 
         @pl.when(valid)
         def _():
-            compute(b)
+            compute(b, part)
 
             @pl.when(at_end & (b != z))
             def _():
-                combine(b)
+                combine(b, part)
 
         return carry
 
-    lax.fori_loop(0, 2 * chips, first_pass, 0)
+    lax.fori_loop(0, 4 * chips, first_pass, 0)
 
     def second_pass(j, carry):
-        b, valid = place_of(j)
+        b, part, valid = place_of(j)
 
         @pl.when(valid & jnp.logical_not(at_end) & (b != z))
         def _():
-            combine(b)
+            combine(b, part)
 
         return carry
 
-    lax.fori_loop(0, 2 * chips, second_pass, 0)
-
-    pair_copy(z).wait_recv()
-    own[z] = own[z] + pair_recv[z].astype(jnp.float32)
-
-    @pl.when(z > 0)
-    def _():
-        right_copy(z).wait_recv()
-        own[z] = own[z] + from_left[z].astype(jnp.float32)
-
-    @pl.when(z + 1 < chips)
-    def _():
-        left_copy(z).wait_recv()
-        own[z] = own[z] + from_right[z].astype(jnp.float32)
-
-    result[...] = (latent[...].astype(jnp.float32) + gate[...] * own[z]).astype(jnp.bfloat16)
-
-    for b in range(chips):
-        pair_copy(b).wait_send()
-
-        @pl.when(b > z)
-        def _():
-            right_copy(b).wait_send()
-
-        @pl.when(b < z)
-        def _():
-            left_copy(b).wait_send()
+    lax.fori_loop(0, 4 * chips, second_pass, 0)
+
+    for part in range(2):
+        u = 2 * z + part
+        cols = slice(part * span, (part + 1) * span)
+        pair_copy(u).wait_recv()
+        own[u] = own[u] + pair_recv[u].astype(jnp.float32)
+
+        @pl.when(z > 0)
+        def _():
+            right_copy(u).wait_recv()
+            own[u] = own[u] + from_left[u].astype(jnp.float32)
+
+        @pl.when(z + 1 < chips)
+        def _():
+            left_copy(u).wait_recv()
+            own[u] = own[u] + from_right[u].astype(jnp.float32)
+
+        result[:, cols] = (latent[:, cols].astype(jnp.float32) + gate[:, cols] * own[u]).astype(
+            jnp.bfloat16
+        )
+
+    for u in range(2 * chips):
+        pair_copy(u).wait_send()
+
+        @pl.when(u // 2 > z)
+        def _():
+            right_copy(u).wait_send()
+
+        @pl.when(u // 2 < z)
+        def _():
+            left_copy(u).wait_send()
 
 
 def tables(places, half):
@@ -664,8 +691,8 @@
             pltpu.VMEM((tp_size, 8, piece), f32),
             pltpu.VMEM((8, width), f32),
             dma((6,)),
-            dma((3, chips)),
-            dma((tp_size,)),
+            dma((3, 2 * chips)),
+            dma((2 * tp_size,)),
             dma((sp_size,)),
             dma((sp_size,)),
             dma((tp_size,)),
@@ -696,7 +723,7 @@
         context_lift,
         head_gain.reshape(1, -1),
     )
-    blocks = (chips, rows, width)
+    blocks = (2 * chips, rows, width // 2)
     return pl.pallas_call(
         functools.partial(output_kernel, tp_size),
         out_shape=jax.ShapeDtypeStruct((rows, width), bf16),
@@ -711,11 +738,11 @@
             pltpu.VMEM(blocks, bf16),
             pltpu.VMEM(blocks, bf16),
             dma(()),
-            dma((chips,)),
-            dma((chips,)),
-            dma((chips,)),
-            dma((chips,)),
-            dma((chips,)),
+            dma((2 * chips,)),
+            dma((2 * chips,)),
+            dma((2 * chips,)),
+            dma((2 * chips,)),
+            dma((2 * chips,)),
         ],
         compiler_params=pltpu.CompilerParams(
             collective_id=1, has_side_effects=True, vmem_limit_bytes=VMEM_LIMIT

time: 125 us -> 122 us (0.976)
  Pallas kernels: 120 us -> 117 us
    pallas_call x1, Pallas kernels: 43.3 us -> 39 us  [shards(): pl.pallas_call(functools.partial(output_kernel, tp_size), out_shape=jax.S...]
where the time goes in v3:
time: 122 us; the launch traced here: 121 us
  Pallas kernels  117 us (96%)
  other arithmetic  2.09 us (2%)
  local copies, waits for them, and re-layouts  1.87 us (2%)
    pallas_call x1, Pallas kernels, shards(): pl.pallas_call(functools.partial(attend_kernel, sp_size, tp_size), out_sh...  78 us
    pallas_call x1, Pallas kernels, shards(): pl.pallas_call(functools.partial(output_kernel, tp_size), out_shape=jax.S...  39 us

profile of v3, /device:TPU:0, one launch (start us, length us, event | category | flops | bytes accessed | tf_op | source)
XLA Modules:
  0.0 121.0 jit_solution(2677286851856377758)
XLA Ops:
  0.0 0.2 broadcast_multiply_fusion.1
  0.2 1.9 %sine_multiply_fusion = (f32[512,128]{1,0:T(8,128)}, f32[512,128]{1,0:T(8,128)}) fusion(f32[128]{0:T(128)S(1)} %compare_select_fusion, f32[512,32]{1,0:T(8,128)S(1)} %get-tuple-element.12, f32[512,32]{1,0:T(8,128)S(1)} %get-tuple-element.11), kind=kLoop, calls=%fused_computation.1 | loop fusion | flops 262144 | bytes 655872 | tf_op jit(solution)/shard_map/mul | solution.py:634
  2.1 78.0 %attend.1 = (bf16[2,512,256]{2,1,0:T(8,128)(2,1)}, f32[1,4096]{1,0:T(1,128)}) custom-call(bf16[64,4096]{1,0:T(8,128)(2,1)} %latent.3, bf16[128,4096]{1,0:T(8,128)(2,1)} %context.1, f32[1,4096]{1,0:T(1,128)} %bitcast.3, f32[1,4096]{1,0:T(1,128)} %bitcast.4, bf16[3,1024,512]{2,1,0:T(8,128)(2,1)} %modulation.1, bf16[4096,512]{1,0:T(8,128)(2,1)} %query_weight.1, ...), custom_call_target="tpu_custom_call" | custom-call | tf_op jit(solution)/shard_map/attend/pallas_call | solution.py:669
  80.1 39.0 %output.1 = bf16[64,4096]{1,0:T(8,128)(2,1)} custom-call(bf16[2,512,256]{2,1,0:T(8,128)(2,1)} %get-tuple-element.7.attended, bf16[512,4096]{1,0:T(8,128)(2,1)} %output_weight.1, bf16[64,4096]{1,0:T(8,128)(2,1)} %latent.3, f32[1,4096]{1,0:T(1,128)} %get-tuple-element.8.gate), custom_call_target="tpu_custom_call" | custom-call | tf_op jit(solution)/shard_map/output/pallas_call | solution.py:727
  119.1 1.9 %copy.14 = bf16[64,4096]{1,0:T(8,128)(2,1)} copy(bf16[64,4096]{1,0:T(8,128)(2,1)} %output.1) | data formatting | bytes 1048576
  (3 shorter events, 0.0 us)
